TPU v7x, 32 devices: a whole 2x2x4 slice. The times are simulated.
32 devices in a mesh: dp: 4 (over y, x), kv: 4 (over z), tp: 2 (over core).
Axes of the slice: x: 2, y: 2, z: 4, core: 2. Of those that a mesh axis runs over, the one named last changes fastest.
Arguments:
- tokens: bfloat16 [64, 4096], P('dp', 'kv'), may hold values from -51 to 51
- norm_gain: float32 [4096], P('kv'), may hold values from 0.1 to 1.9
- w_query: bfloat16 [4096, 2048], P('kv', 'tp'), may hold values from -0.09375 to 0.09375
- lambda_head: float32 [16], P('tp'), may hold values from 0.3 to 0.8
- head_gain: float32 [128], replicated, may hold values from 0.1 to 1.9
- w_out: bfloat16 [2048, 4096], P('tp', 'kv'), may hold values from -0.125 to 0.125
- rotated_key_cache: bfloat16 [64, 1024, 128], P('dp', 'kv'), may hold values from -540 to 540, as said below
- value_cache: bfloat16 [64, 1024, 128], P('dp', 'kv'), may hold values from -6 to 6
- lengths: int32 [64], P('dp'), may hold values from 256 to 1024
Outputs:
- mixed: bfloat16 [64, 4096], P('dp', ('kv', 'tp'))
Inputs may be any that keep to these rules, and one draw needn't show every extreme that they name: `rotated_key_cache`: keys have an order-one typical size. The new token is the last filled position, lengths - 1.
All inputs are finite; a program needn't handle non-finite values.
Results may differ from a plain program's by a relative error of at most 0.0112.
Values may be sent and summed in bfloat16 or wider, within the bound.
No kernel may reach another device: no remote copies, remote signals or barrier semaphores. Data moves between devices by JAX's collectives and lax.ppermute only.
A program may use at most 64 MiB of HBM per device.

v0:
```python
import jax
import jax.numpy as jnp
from jax import lax
from jax.sharding import PartitionSpec as P

D = 4096
HEAD_FEATURES = 64
VALUE_DIM = 128


EPS = 1e-05


def combined_all(part, axis, combine):
    gathered = jax.tree.map(lambda a: lax.all_gather(a, axis), part)

    def take(source):
        return jax.tree.map(lambda a: lax.dynamic_index_in_dim(a, source, 0, False), gathered)

    return lax.fori_loop(
        1, lax.axis_size(axis), lambda source, state: combine(state, take(source)), take(0)
    )


def rotate_query(query, position):
    half_dim = query.shape[-1] // 2
    frequency = 1.0 / 10000.0 ** (jnp.arange(half_dim, dtype=jnp.float32) / half_dim)
    angles = position[:, None] * frequency[None, :]
    cosine_table = jnp.concatenate([jnp.cos(angles), jnp.cos(angles)], -1)[:, None, None, :]
    sine_table = jnp.concatenate([jnp.sin(angles), jnp.sin(angles)], -1)[:, None, None, :]
    first_half = query[..., :half_dim]
    second_half = query[..., half_dim:]
    turned = jnp.concatenate([-second_half, first_half], -1)
    return query * cosine_table + turned * sine_table


def finish(numerators, totals, lambdas, head_gain):
    averaged = numerators / totals[..., None]
    head_result = averaged[..., 0, :] - lambdas[..., None] * averaged[..., 1, :]
    factor = lax.rsqrt(jnp.mean(head_result * head_result, -1, keepdims=True) + EPS)
    return (head_result * factor * head_gain).astype(jnp.bfloat16)


def combine_blocks(earlier, later):
    top = jnp.maximum(earlier[0], later[0])
    first_factor = jnp.exp(earlier[0] - top)
    second_factor = jnp.exp(later[0] - top)
    totals = earlier[1] * first_factor + later[1] * second_factor
    numerators = earlier[2] * first_factor[..., None] + later[2] * second_factor[..., None]
    return (top, totals, numerators)


def on_device(
    tokens,
    norm_gain,
    w_query,
    lambda_head,
    head_gain,
    w_out,
    rotated_key_cache,
    value_cache,
    lengths,
):
    seq_count = tokens.shape[0]
    head_count = lambda_head.shape[0]
    pos_count = rotated_key_cache.shape[1]
    widened = tokens.astype(jnp.float32)
    squares = jnp.sum(widened * widened, -1)
    scaled_in = (widened * norm_gain).astype(jnp.bfloat16)
    partial_query = jnp.dot(scaled_in, w_query, preferred_element_type=jnp.float32)
    squares = lax.psum(squares, "kv")
    raw_query = lax.psum(partial_query, "kv")
    scale_rows = lax.rsqrt(squares / D + EPS)
    shaped = (raw_query * scale_rows[:, None]).reshape(seq_count, head_count, 2, HEAD_FEATURES)
    query = rotate_query(shaped, (lengths - 1).astype(jnp.float32))
    keys = rotated_key_cache.reshape(seq_count, pos_count, 2, HEAD_FEATURES)
    score_rows = jnp.einsum(
        "bhmd,bpmd->bhmp",
        query,
        keys,
        preferred_element_type=jnp.float32,
        precision=lax.Precision.HIGHEST,
    ) * HEAD_FEATURES ** (-0.5)
    position_list = lax.axis_index("kv") * pos_count + jnp.arange(pos_count, dtype=jnp.int32)
    valid = (position_list[None, :] < lengths[:, None])[:, None, None, :]
    masked = jnp.where(valid, score_rows, -1e30)
    maxima = jnp.max(masked, -1)
    weights = jnp.where(valid, jnp.exp(masked - maxima[..., None]), 0.0)
    totals = jnp.sum(weights, -1)
    numerators = jnp.einsum(
        "bhmp,bpv->bhmv",
        weights.astype(jnp.bfloat16),
        value_cache,
        preferred_element_type=jnp.float32,
    )
    merged = combined_all((maxima, totals, numerators), "kv", combine_blocks)
    normed = finish(merged[2], merged[1], lambda_head[None, :], head_gain).reshape(
        seq_count, head_count * VALUE_DIM
    )
    projected = jnp.dot(normed, w_out, preferred_element_type=jnp.float32)
    return lax.psum_scatter(projected, "tp", scatter_dimension=1, tiled=True).astype(jnp.bfloat16)


def solution(mesh):
    in_specs = (
        P("dp", "kv"),
        P("kv"),
        P("kv", "tp"),
        P("tp"),
        P(),
        P("tp", "kv"),
        P("dp", "kv", None),
        P("dp", "kv", None),
        P("dp"),
    )
    out_specs = P("dp", ("kv", "tp"))
    return jax.shard_map(
        on_device, mesh=mesh, in_specs=in_specs, out_specs=out_specs, check_vma=False
    )
```

profile of v0, /device:TPU:0, one launch (start us, length us, event | category | flops | bytes accessed | tf_op | source)
XLA Modules:
  0.0 114.8 jit_solution(7172652897911853085)
XLA Ops:
  6.6 1.5 %copy-done = bf16[1024,1024]{1,0:T(8,128)(2,1)S(1)} copy-done((bf16[1024,1024]{1,0:T(8,128)(2,1)S(1)}, bf16[1024,1024]{1,0:T(8,128)(2,1)}, u32[]{:S(2)}) %copy-start) | copy-done | bytes 2097176
  8.1 1.8 %fusion.28 = f32[16,1024]{1,0:T(8,128)} fusion(bf16[1024,1024]{1,0:T(8,128)(2,1)S(1)} %copy-done, bf16[16,1024]{1,0:T(8,128)(2,1)} %param.11, f32[1024]{0:T(1024)} %param.12), kind=kOutput, calls=%fused_computation.41 | convolution fusion | flops 33603584 | bytes 2199552 | tf_op jit(solution)/shard_map/dot_general | solution.py:70
  10.0 0.1 fusion.20
  10.1 13.5 %psum.15 = f32[16]{0:T(128)S(1)} all-reduce(f32[16]{0:T(128)S(1)} %fusion.20), channel_id=1, replica_groups=mesh['dp'=4,'kv'=4,'tp'=2] {'kv'}, use_global_device_ids=true, to_apply=%region_2.0 | all-reduce | flops 16 | bytes 128 | tf_op jit(solution)/shard_map/psum | solution.py:71
  23.7 1.5 %copy.41 = bf16[16,256,128]{1,2,0:T(8,128)(2,1)S(1)} copy(bf16[16,256,128]{2,1,0:T(8,128)(2,1)} %param.17) | data formatting | bytes 2097152 | tf_op args[6]
  25.2 0.1 multiply_cosine_fusion
  25.5 21.6 %all-reduce.2.cloned.1.call-done = f32[16,1024]{1,0:T(8,128)} async-done(((f32[16,1024]{1,0:T(8,128)}), f32[16,1024]{1,0:T(8,128)}) %all-reduce.2.cloned.1.call-update) | async-done | bytes 65552 | tf_op jit(solution)/shard_map/psum | solution.py:72
  47.1 0.9 broadcast_multiply_fusion
  48.0 0.1 reshape.64
  48.3 0.7 fusion.37
  49.0 13.2 %all-gather = f32[64,8,2]{1,2,0:T(2,128)S(1)} all-gather(f32[16,8,2]{1,2,0:T(2,128)S(1)} %get-tuple-element.230), channel_id=2, replica_groups=mesh['dp'=4,'kv'=4,'tp'=2] {'kv'}, dimensions={0}, use_global_device_ids=true | all-gather | bytes 5120 | tf_op jit(solution)/shard_map/all_gather | solution.py:15
  62.1 0.2 fusion.9
  62.4 0.3 fusion.6
  62.7 15.8 %all-gather.2 = f32[64,8,2,128]{3,1,2,0:T(8,128)S(1)} all-gather(f32[16,8,2,128]{3,1,2,0:T(8,128)S(1)} %fusion.6), channel_id=4, replica_groups=mesh['dp'=4,'kv'=4,'tp'=2] {'kv'}, dimensions={0}, use_global_device_ids=true | all-gather | bytes 655360 | tf_op jit(solution)/shard_map/all_gather | solution.py:15
  78.5 13.1 %all-gather.1 = f32[64,8,2]{1,2,0:T(2,128)S(1)} all-gather(f32[16,8,2]{1,2,0:T(2,128)S(1)} %fusion.9), channel_id=3, replica_groups=mesh['dp'=4,'kv'=4,'tp'=2] {'kv'}, dimensions={0}, use_global_device_ids=true | all-gather | bytes 5120 | tf_op jit(solution)/shard_map/all_gather | solution.py:15
  92.0 3.4 %while.19 = (s32[]{:T(128)}, f32[16,8,2]{0,2,1:T(2,128)S(1)}, f32[16,8,2]{0,2,1:T(2,128)S(1)}, f32[16,8,2,128]{3,2,1,0:T(2,128)S(1)}, f32[4,16,8,2]{1,3,2,0:T(2,...) while((s32[]{:T(128)}, f32[16,8,2]{0,2,1:T(2,128)S(1)}, ...), condition=%wide.region_6.7_spmd, body=%wide.region_5.6_spmd.sunk | while | flops 99845 | bytes 669847 | solution.py:20
  92.1 0.1 copy.83
  92.2 0.1 copy.84
  92.3 0.8 fusion.44
  93.2 0.1 copy.83
  93.3 0.1 copy.84
  93.5 0.8 fusion.44
  94.3 0.1 copy.83
  94.5 0.1 copy.84
  94.6 0.8 fusion.44
  95.4 0.1 copy.50
  95.5 0.2 broadcast_divide_fusion
  95.8 0.2 slice_reduce_fusion
  96.0 0.2 multiply_reduce_fusion
  96.3 2.6 %fusion.26 = f32[16,1024]{1,0:T(8,128)} fusion(bf16[1024,1024]{1,0:T(8,128)(2,1)} %param.16, f32[2,8,8,128]{3,2,1,0:T(8,128)S(1)} %bitcast.72, f32[2,8,8,128]{3,2,1,0:T(8,128)S(1)} %bitcast.71, f32[2,8,8,128]{3,2,1,0:T(8,128)S(1)} %bitcast.68, f32[1024]{0:T(1024)S(1)} %get-tuple-element.234, f32[1024]{0:T(1024)S(1)} %get-tuple-element.235), kind=kOutput, calls=%fused_computation.40 | convolution fusion | flops 33636352 | bytes 2367488 | tf_op jit(solution)/shard_map/dot_general | solution.py:100
  98.9 7.8 %reduce-scatter.2.cloned.1.call-done = f32[16,512]{1,0:T(8,128)} async-done(((f32[16,1024]{1,0:T(8,128)}), f32[16,512]{1,0:T(8,128)}) %reduce-scatter.2.cloned.1.call-update) | async-done | bytes 32784 | tf_op jit(solution)/shard_map/reduce_scatter | solution.py:101
  106.6 1.4 %convert_element_type.24 = bf16[16,512]{1,0:T(8,128)(2,1)} convert(f32[16,512]{1,0:T(8,128)} %reduce-scatter.2.cloned.1.call-done) | non-fusion elementwise | flops 8192 | bytes 49152 | tf_op jit(solution)/shard_map/convert_element_type | solution.py:101
  (40 shorter events, 1.2 us)
Async XLA Ops:
  6.5 1.6 %copy-start = (bf16[1024,1024]{1,0:T(8,128)(2,1)S(1)}, bf16[1024,1024]{1,0:T(8,128)(2,1)}, u32[]{:S(2)}) copy-start(bf16[1024,1024]{1,0:T(8,128)(2,1)} %param.13) | copy-start | bytes 6291460
  6.5 3.4 %copy-start.1 = (bf16[16,1024]{1,0:T(8,128)(2,1)S(1)}, bf16[16,1024]{1,0:T(8,128)(2,1)}, u32[]{:S(2)}) copy-start(bf16[16,1024]{1,0:T(8,128)(2,1)} %param.11) | copy-start | bytes 98308
  6.5 3.6 %copy-start.4 = (s32[16]{0:T(128)S(1)}, s32[16]{0:T(128)}, u32[]{:S(2)}) copy-start(s32[16]{0:T(128)} %param.19) | copy-start | bytes 196
  6.5 18.8 %copy-start.2 = (f32[8]{0:T(128)S(1)}, f32[8]{0:T(128)}, u32[]{:S(2)}) copy-start(f32[8]{0:T(128)} %param.14) | copy-start | bytes 100
  6.5 18.8 %copy-start.3 = (f32[128]{0:T(128)S(1)}, f32[128]{0:T(128)}, u32[]{:S(2)}) copy-start(f32[128]{0:T(128)} %param.15) | copy-start | bytes 1540
  6.5 40.6 %all-reduce.2.cloned.1.call-start = ((), (), s32[]{:S(2)}) async-start(), calls=%async_computation.1 | async-start | bytes 131072 | tf_op jit(solution)/shard_map/psum | solution.py:72
  9.9 96.7 %reduce-scatter.2.cloned.1.call-start = ((), (), s32[]{:S(2)}) async-start(), calls=%async_computation.2 | async-start | bytes 98304 | tf_op jit(solution)/shard_map/reduce_scatter | solution.py:101
  48.2 14.2 %copy-start.5 = (bf16[16,256,128]{2,1,0:T(8,128)(2,1)S(1)}, bf16[16,256,128]{2,1,0:T(8,128)(2,1)}, u32[]{:S(2)}) copy-start(bf16[16,256,128]{2,1,0:T(8,128)(2,1)} %param.18) | copy-start | bytes 3145732
Sparse Core Ops, SparseCore 0:
  10.0 37.0 all-reduce.1
  99.0 7.5 reduce-scatter.1
where the time goes:
time: 115 us
  blocking collectives  55.5 us (48%)
  waiting for transfers between devices  29.4 us (26%)
  between operations  13.6 us (12%)
  other arithmetic  5.9 us (5%)
  matrix products  5.38 us (5%)
  local copies, waits for them, and re-layouts  4.94 us (4%)
    all_gather x3, blocking collectives, combined_all(): gathered = jax.tree.map(lambda a: lax.all_gather(a, axis), part)  42 us
    psum x1, waiting for transfers between devices, on_device(): raw_query = lax.psum(partial_query, 'kv')  21.6 us
    psum x1, blocking collectives, on_device(): squares = lax.psum(squares, 'kv')  13.5 us
    reduce_scatter x1, waiting for transfers between devices, on_device(): lax.psum_scatter(projected, 'tp', scatter_dimension=1, tiled=True)  7.75 us
    unnamed x13, local copies, waits for them, and re-layouts  3.04 us
    dot_general x1, matrix products, on_device(): projected = jnp.dot(normed, w_out, preferred_element_type=jnp.float32)  2.61 us
    add x3, other arithmetic, combine_blocks(): earlier[2] * first_factor[..., None] + later[2] * second_factor[..., None]  2.39 us
  transfers between devices with their start and end apart: 2, of which 2 were waited for; matrix products, arithmetic and copies ran while one was open for 2% of the time, Pallas kernels for 0%

commit v1 on v0

v1 whole, which is shorter than its diff:
```python
import functools

import jax
import jax.numpy as jnp
from jax import lax
from jax.experimental import pallas as pl
from jax.experimental.pallas import tpu as pltpu
from jax.sharding import PartitionSpec as P


HEAD_FEATURES = 64
VALUE_DIM = 128
LANES = 128
EPS = 1e-05
ROPE_BASE = 10000.0
MASKED = -1e30
F32 = jnp.float32
BF16 = jnp.bfloat16
VMEM = pl.BlockSpec(memory_space=pltpu.VMEM)
SMEM = pl.BlockSpec(memory_space=pltpu.SMEM)


def lane_index(shape):
    return lax.broadcasted_iota(jnp.int32, shape, len(shape) - 1)


def split3(x):
    high = x.astype(BF16).astype(F32)
    rest = x - high
    middle = rest.astype(BF16).astype(F32)
    return high, middle, (rest - middle).astype(BF16).astype(F32)


def project_kernel(tokens_ref, gain_ref, weights_ref, out_ref):
    heads = out_ref.shape[0] - 1
    widened = tokens_ref[...].astype(F32)
    squares = jnp.sum(widened * widened, -1, keepdims=True)
    scaled = (widened * gain_ref[...]).astype(BF16)
    part = jnp.dot(scaled, weights_ref[...], preferred_element_type=F32)
    for head in range(heads):
        out_ref[head] = part[:, head * LANES : (head + 1) * LANES]
    out_ref[heads] = jnp.broadcast_to(squares, out_ref.shape[1:])


def attend_kernel(width, count, limits_ref, *refs):
    parts, (cosine_ref, sine_ref, keys_ref, values_ref, out_ref, query_ref) = refs[:count], refs[count:]
    heads = parts[0].shape[0] - 1
    seqs, positions = keys_ref.shape[:2]

    def summed(index):
        total = parts[0][index]
        for part in parts[1:]:
            total = total + part[index]
        return total

    scale = lax.rsqrt(summed(heads) / width + EPS) * HEAD_FEATURES ** (-0.5)
    cosine, sine = cosine_ref[...] * scale, sine_ref[...] * scale
    half = HEAD_FEATURES // 2
    low = (lane_index(cosine.shape) % HEAD_FEATURES) < half
    for head in range(heads):
        raw = summed(head)
        turned = jnp.where(low, pltpu.roll(raw, LANES - half, 1), pltpu.roll(raw, half, 1))
        query_ref[:, head, :] = raw * cosine + turned * sine

    first = lane_index((heads, LANES)) < HEAD_FEATURES
    rows = 2 * heads
    lanes = lane_index((rows, LANES))
    places = lane_index((rows, positions))
    maxima = jnp.zeros((rows, LANES), F32)
    totals = jnp.zeros((rows, LANES), F32)
    for seq in range(seqs):
        pieces = split3(query_ref[seq])
        left = jnp.concatenate(
            [jnp.where(keep, piece, 0.0) for piece in pieces for keep in (first, ~first)], 0
        ).astype(BF16)
        products = lax.dot_general(
            left, keys_ref[seq], (((1,), (1,)), ((), ())), preferred_element_type=F32
        )
        scores = products[:rows] + (products[rows : 2 * rows] + products[2 * rows :])
        valid = places < limits_ref[seq]
        masked = jnp.where(valid, scores, MASKED)
        top = jnp.max(masked, -1, keepdims=True)
        weights = jnp.where(valid, jnp.exp(masked - top), 0.0)
        maxima = jnp.where(lanes == seq, top, maxima)
        totals = jnp.where(lanes == seq, jnp.sum(weights, -1, keepdims=True), totals)
        out_ref[seq] = jnp.dot(
            weights.astype(BF16), values_ref[seq], preferred_element_type=F32
        ).astype(BF16)
    packed = jnp.zeros((rows, LANES), F32)
    for place, piece in enumerate(split3(maxima) + split3(totals)):
        inside = (lanes >= place * seqs) & (lanes < (place + 1) * seqs)
        moved = pltpu.roll(piece, place * seqs, 1) if place else piece
        packed = jnp.where(inside, moved, packed)
    out_ref[seqs] = packed.astype(BF16)


def combine(parts, signs_ref, gain_ref, mixed_ref):
    seqs, rows = parts[0].shape[0] - 1, parts[0].shape[1]
    heads = rows // 2

    def unpacked(part, place):
        packed = part[seqs].astype(F32)
        total = None
        for piece in range(place, place + 3):
            moved = pltpu.roll(packed, LANES - piece * seqs, 1) if piece else packed
            total = moved if total is None else total + moved
        return total

    maxima = [unpacked(part, 0) for part in parts]
    top = functools.reduce(jnp.maximum, maxima)
    factors = [jnp.exp(own - top) for own in maxima]
    totals = sum(factor * unpacked(part, 3) for factor, part in zip(factors, parts))
    shares = signs_ref[...] / totals
    factors = [factor * shares for factor in factors]
    gain = gain_ref[...]
    for seq in range(seqs):
        both = sum(
            factor[:, seq : seq + 1] * part[seq].astype(F32) for factor, part in zip(factors, parts)
        )
        head_out = both[:heads] + both[heads:]
        mean = jnp.mean(head_out * head_out, -1, keepdims=True)
        mixed_ref[seq] = head_out * lax.rsqrt(mean + EPS) * gain


def finish_kernel(count, side_ref, *refs):
    parts = refs[:count]
    signs_ref, gain_ref, weights_ref, normed_ref, sent_ref, mixed_ref = refs[count:]
    combine(parts, signs_ref, gain_ref, mixed_ref)
    for head in range(mixed_ref.shape[1]):
        normed_ref[:, head * VALUE_DIM : (head + 1) * VALUE_DIM] = mixed_ref[:, head, :].astype(BF16)
    width = sent_ref.shape[1]
    start = pl.multiple_of((1 - side_ref[0]) * width, width)
    sent_ref[...] = jnp.dot(
        normed_ref[...], weights_ref[:, pl.ds(start, width)], preferred_element_type=F32
    )


def own_kernel(side_ref, normed_ref, weights_ref, out_ref):
    width = out_ref.shape[1]
    start = pl.multiple_of(side_ref[0] * width, width)
    out_ref[...] = jnp.dot(
        normed_ref[...], weights_ref[:, pl.ds(start, width)], preferred_element_type=F32
    )


def call(kernel, out_shape, in_specs, scratch=(), flops=0):
    out_specs = jax.tree.map(lambda _: VMEM, out_shape)
    return pl.pallas_call(
        kernel,
        out_shape=out_shape,
        in_specs=in_specs,
        out_specs=out_specs,
        scratch_shapes=scratch,
        cost_estimate=pl.CostEstimate(flops=flops, bytes_accessed=1 << 20, transcendentals=0),
    )


def exchanged(x, axis):
    count = lax.axis_size(axis)
    received = []
    for step in range(count - 1, 0, -1):
        pairs = [(source, source ^ step) for source in range(count)]
        received.append(lax.ppermute(x, axis, pairs))
    return [x] + received


def tables(lengths, copies):
    half = HEAD_FEATURES // 2
    frequency = 1.0 / ROPE_BASE ** (jnp.arange(half, dtype=F32) / half)
    angles = (lengths - 1).astype(F32)[:, None] * frequency[None, :]
    cosine, sine = jnp.cos(angles), jnp.sin(angles)
    return (
        jnp.concatenate([cosine, cosine] * copies, -1),
        jnp.concatenate([-sine, sine] * copies, -1),
    )


def near_device(
    tokens, norm_gain, w_query, lambda_head, head_gain, w_out, rotated_key_cache, value_cache, lengths
):
    seqs, features = tokens.shape
    heads = lambda_head.shape[0]
    positions = rotated_key_cache.shape[1]
    count = lax.axis_size("kv")
    cosine, sine = tables(lengths, LANES // HEAD_FEATURES)
    limits = lengths - lax.axis_index("kv").astype(jnp.int32) * positions
    side = lax.axis_index("tp").astype(jnp.int32).reshape(1)
    signs = jnp.broadcast_to(
        jnp.concatenate([jnp.ones_like(lambda_head), -lambda_head])[:, None], (2 * heads, LANES)
    )

    partial = call(
        project_kernel,
        jax.ShapeDtypeStruct((heads + 1, seqs, LANES), F32),
        [VMEM] * 3,
        flops=2 * seqs * features * heads * LANES,
    )(tokens, norm_gain[None, :], w_query)
    queries = exchanged(partial, "kv")

    blocks = call(
        functools.partial(attend_kernel, features * count, count),
        jax.ShapeDtypeStruct((seqs + 1, 2 * heads, LANES), BF16),
        [SMEM] + [VMEM] * (count + 4),
        [pltpu.VMEM((seqs, heads, LANES), F32)],
        flops=8 * seqs * heads * positions * LANES,
    )(limits, *queries, cosine, sine, rotated_key_cache, value_cache)
    gathered = exchanged(blocks, "kv")

    columns = w_out.shape[1] // 2
    flops = 2 * seqs * heads * VALUE_DIM * columns
    normed, sent = call(
        functools.partial(finish_kernel, count),
        (
            jax.ShapeDtypeStruct((seqs, heads * VALUE_DIM), BF16),
            jax.ShapeDtypeStruct((seqs, columns), F32),
        ),
        [SMEM] + [VMEM] * (count + 3),
        [pltpu.VMEM((seqs, heads, LANES), F32)],
        flops=flops,
    )(side, *gathered, signs, head_gain[None, :], w_out)
    received = lax.ppermute(sent, "tp", [(0, 1), (1, 0)])
    own = call(
        own_kernel, jax.ShapeDtypeStruct((seqs, columns), F32), [SMEM, VMEM, VMEM], flops=flops
    )(side, normed, w_out)
    return (own + received).astype(BF16)


def far_device(
    tokens, norm_gain, w_query, lambda_head, head_gain, w_out, rotated_key_cache, value_cache, lengths
):
    seqs, features = tokens.shape
    heads = lambda_head.shape[0]
    positions = rotated_key_cache.shape[1]
    widened = tokens.astype(F32)
    scaled = (widened * norm_gain).astype(BF16)
    squares = lax.psum(jnp.sum(widened * widened, -1), "kv")
    raw = lax.psum(jnp.dot(scaled, w_query, preferred_element_type=F32), "kv")
    scale = lax.rsqrt(squares / (features * lax.axis_size("kv")) + EPS)
    raw = (raw * scale[:, None]).reshape(seqs, heads, 2, HEAD_FEATURES)
    cosine, sine = tables(lengths, 1)
    turned = jnp.roll(raw, HEAD_FEATURES // 2, -1)
    query = raw * cosine[:, None, None, :] + turned * sine[:, None, None, :]
    keys = rotated_key_cache.reshape(seqs, positions, 2, HEAD_FEATURES)
    scores = jnp.einsum(
        "bhmd,bpmd->bhmp", query, keys, preferred_element_type=F32, precision=lax.Precision.HIGHEST
    ) * HEAD_FEATURES ** (-0.5)
    places = lax.axis_index("kv") * positions + jnp.arange(positions, dtype=jnp.int32)
    valid = (places[None, :] < lengths[:, None])[:, None, None, :]
    masked = jnp.where(valid, scores, MASKED)
    top = lax.pmax(jnp.max(masked, -1), "kv")
    weights = jnp.where(valid, jnp.exp(masked - top[..., None]), 0.0)
    totals = lax.psum(jnp.sum(weights, -1), "kv")
    numerators = lax.psum(
        jnp.einsum("bhmp,bpv->bhmv", weights.astype(BF16), value_cache, preferred_element_type=F32), "kv"
    )
    averaged = numerators / totals[..., None]
    head_out = averaged[..., 0, :] - lambda_head[None, :, None] * averaged[..., 1, :]
    factor = lax.rsqrt(jnp.mean(head_out * head_out, -1, keepdims=True) + EPS)
    normed = (head_out * factor * head_gain).astype(BF16).reshape(seqs, heads * VALUE_DIM)
    projected = jnp.dot(normed, w_out, preferred_element_type=F32)
    return lax.psum_scatter(projected, "tp", scatter_dimension=1, tiled=True).astype(BF16)


def solution(mesh):
    count = mesh.shape["kv"]
    near = count <= 4 and count & (count - 1) == 0 and mesh.shape["tp"] == 2
    in_specs = (
        P("dp", "kv"),
        P("kv"),
        P("kv", "tp"),
        P("tp"),
        P(),
        P("tp", "kv"),
        P("dp", "kv", None),
        P("dp", "kv", None),
        P("dp"),
    )
    return jax.shard_map(
        near_device if near else far_device,
        mesh=mesh,
        in_specs=in_specs,
        out_specs=P("dp", ("kv", "tp")),
        check_vma=False,
    )
```

time: 115 us -> 38.6 us (0.34)
  blocking collectives: 55.5 us -> 0 us
  waiting for transfers between devices: 29.4 us -> 9.29 us
  Pallas kernels: 0 us -> 14.8 us
  between operations: 13.6 us -> 0.03 us
  starting transfers between devices: 0.08 us -> 10 us
  matrix products: 5.38 us -> 0 us
  local copies, waits for them, and re-layouts: 4.94 us -> 1.42 us
  other arithmetic: 5.9 us -> 2.71 us
    all_gather x3 -> x0, blocking collectives: 42 us -> none  [combined_all(): gathered = jax.tree.map(lambda a: lax.all_gather(a, axis), part)]
    psum x1 -> x0, waiting for transfers between devices: 21.6 us -> none  [on_device(): raw_query = lax.psum(partial_query, 'kv')]
    pallas_call x0 -> x4, Pallas kernels: none -> 14.8 us  [the longest x1 6.55 us: near_device(): call(functools.partial(attend_kernel, features * count, count), jax.Shape...]
    psum x1 -> x0, blocking collectives: 13.5 us -> none  [on_device(): squares = lax.psum(squares, 'kv')]
    ppermute x0 -> x7, starting transfers between devices: none -> 10 us  [the longest x6 10 us: exchanged(): received.append(lax.ppermute(x, axis, pairs))]
    ppermute x0 -> x7, waiting for transfers between devices: none -> 9.29 us  [the longest x6 9.28 us: exchanged(): received.append(lax.ppermute(x, axis, pairs))]
    reduce_scatter x1 -> x0, waiting for transfers between devices: 7.75 us -> none  [on_device(): lax.psum_scatter(projected, 'tp', scatter_dimension=1, tiled=True)]
    dot_general x4 -> x0, matrix products: 5.38 us -> none  [the longest x1 2.61 us: on_device(): projected = jnp.dot(normed, w_out, preferred_element_type=jnp.float32)]
  transfers between devices with their start and end apart: 2 -> 7, of which waited for: 2 -> 4; matrix products, arithmetic and copies ran while one was open for 2% -> 4% of each run, Pallas kernels for 0% -> 6%
where the time goes in v1:
time: 38.6 us; the launch traced here: 38.3 us
  Pallas kernels  14.8 us (38%)
  starting transfers between devices  10 us (26%)
  waiting for transfers between devices  9.29 us (24%)
  other arithmetic  2.71 us (7%)
  local copies, waits for them, and re-layouts  1.42 us (4%)
    ppermute x6, starting transfers between devices, exchanged(): received.append(lax.ppermute(x, axis, pairs))  10 us
    ppermute x6, waiting for transfers between devices, exchanged(): received.append(lax.ppermute(x, axis, pairs))  9.28 us
    pallas_call x1, Pallas kernels, near_device(): call(functools.partial(attend_kernel, features * count, count), jax.Shape...  6.55 us
    pallas_call x1, Pallas kernels, near_device(): call(functools.partial(finish_kernel, count), (jax.ShapeDtypeStruct((seqs...  3.13 us
    pallas_call x1, Pallas kernels, near_device(): call(project_kernel, jax.ShapeDtypeStruct((heads + 1, seqs, LANES), F32),...  2.69 us
    pallas_call x1, Pallas kernels, near_device(): call(own_kernel, jax.ShapeDtypeStruct((seqs, columns), F32), [SMEM, VMEM,...  2.48 us
    convert_element_type x1, other arithmetic, near_device(): return (own + received).astype(BF16)  1.37 us
  transfers between devices with their start and end apart: 7, of which 4 were waited for; matrix products, arithmetic and copies ran while one was open for 4% of the time, Pallas kernels for 6%

profile of v1, /device:TPU:0, one launch (start us, length us, event | category | flops | bytes accessed | tf_op | source)
XLA Modules:
  0.0 38.3 jit_solution(18404069126377618172)
XLA Ops:
  0.0 2.7 %shard_map.91.refs_0_ = f32[9,16,128]{2,1,0:T(8,128)} custom-call(bf16[16,1024]{1,0:T(8,128)(2,1)} %tokens_ref.1, f32[1,1024]{1,0:T(1,128)} %bitcast.3, bf16[1024,1024]{1,0:T(8,128)(2,1)} %weights_ref.2), custom_call_target="tpu_custom_call" | custom-call | flops 33554432 | bytes 1048576 | tf_op jit(solution)/shard_map/pallas_call | solution.py:192
  2.7 5.1 %collective-permute-start = (f32[9,16,128]{2,1,0:T(8,128)}, f32[9,16,128]{2,1,0:T(8,128)S(1)}, u32[]{:S(2)}, u32[]{:S(2)}) collective-permute-start(f32[9,16,128]{2,1,0:T(8,128)} %shard_map.91.refs_0_), channel_id=1, source_target_pairs={{0,6},{2,4},{4,2},{6,0},{1,7},{3,5},{5,3},{7,1},{8,14},{10,12},{12... | collective-permute-start | bytes 221192 | tf_op jit(solution)/shard_map/ppermute | solution.py:163
  7.8 0.0 collective-permute-start.1
  7.8 0.6 %collective-permute-start.2 = (f32[9,16,128]{2,1,0:T(8,128)}, f32[9,16,128]{2,1,0:T(8,128)S(1)}, u32[]{:S(2)}, u32[]{:S(2)}) collective-permute-start(f32[9,16,128]{2,1,0:T(8,128)} %shard_map.91.refs_0_), channel_id=1, source_target_pairs={{0,2},{2,0},{4,6},{6,4},{1,3},{3,1},{5,7},{7,5},{8,10},{10,8},{12,... | collective-permute-start | bytes 221192 | tf_op jit(solution)/shard_map/ppermute | solution.py:163
  8.3 0.0 copy-done.6
  8.3 0.5 %add_convert_fusion.1 = (f32[16]{0:T(128)S(1)}, s32[16]{0:T(128)}) fusion(s32[16]{0:T(128)S(1)} %copy-done.6, s32[]{:T(128)S(6)} %mul.16), kind=kLoop, calls=%fused_computation.7 | loop fusion | flops 48 | bytes 196 | tf_op jit(solution)/shard_map/convert_element_type | solution.py:170
  8.9 0.1 fusion
  9.0 0.7 %pad_maximum_fusion = (f32[16,128]{1,0:T(8,128)}, f32[16,128]{1,0:T(8,128)}) fusion(f32[16,32]{1,0:T(8,128)S(1)} %get-tuple-element.11, f32[16,32]{1,0:T(8,128)S(1)} %get-tuple-element.10, f32[16,32]{1,0:T(8,128)S(1)} %get-tuple-element.9), kind=kLoop, calls=%fused_computation.3 | loop fusion | flops 12288 | bytes 22528 | tf_op jit(solution)/shard_map/concatenate | solution.py:173
  9.7 1.1 %collective-permute-done.refs_1_ = f32[9,16,128]{2,1,0:T(8,128)S(1)} collective-permute-done((f32[9,16,128]{2,1,0:T(8,128)}, f32[9,16,128]{2,1,0:T(8,128)S(1)}, u32[]{:S(2)}, u32[]{:S(2)}) %collective-permute-start) | collective-permute-done | bytes 73760 | tf_op jit(solution)/shard_map/ppermute | solution.py:163
  10.7 3.4 %collective-permute-done.1.refs_2_ = f32[9,16,128]{2,1,0:T(8,128)S(1)} collective-permute-done((f32[9,16,128]{2,1,0:T(8,128)}, f32[9,16,128]{2,1,0:T(8,128)S(1)}, u32[]{:S(2)}, u32[]{:S(2)}) %collective-permute-start.1) | collective-permute-done | bytes 73760 | tf_op jit(solution)/shard_map/ppermute | solution.py:163
  14.2 0.0 collective-permute-done.2.refs_3_
  14.2 0.0 copy-done
  14.2 0.6 %copy-done.1 = f32[9,16,128]{2,1,0:T(8,128)} copy-done((f32[9,16,128]{2,1,0:T(8,128)}, f32[9,16,128]{2,1,0:T(8,128)S(1)}, u32[]{:S(2)}) %copy-start.1) | copy-done | bytes 73752
  14.8 0.0 copy-done.2
  14.9 6.6 %shard_map.92.refs_0_ = bf16[17,16,128]{2,1,0:T(8,128)(2,1)} custom-call(s32[16]{0:T(128)} %get-tuple-element.13.limits_ref, f32[9,16,128]{2,1,0:T(8,128)} %shard_map.91.refs_0_, f32[9,16,128]{2,1,0:T(8,128)} %copy-done, f32[9,16,128]{2,1,0:T(8,128)} %copy-done.1, f32[9,16,128]{2,1,0:T(8,128)} %copy-done.2, f32[16,128]{1,0:T(8,128)} %get-tuple-element.14.refs_4_, ...), custom_call_target="tpu_custom_call" | custom-call | flops 33554432 | bytes 1048576 | tf_op jit(solution)/shard_map/pallas_call | solution.py:200
  21.4 2.6 %collective-permute-start.3 = (bf16[17,16,128]{2,1,0:T(8,128)(2,1)}, bf16[17,16,128]{2,1,0:T(8,128)(2,1)S(1)}, u32[]{:S(2)}, u32[]{:S(2)}) collective-permute-start(bf16[17,16,128]{2,1,0:T(8,128)(2,1)} %shard_map.92.refs_0_), channel_id=1, source_target_pairs={{0,6},{2,4},{4,2},{6,0},{1,7},{3,5},{5,3},{7,1},{8,14},{10,12},{12... | collective-permute-start | bytes 208904 | tf_op jit(solution)/shard_map/ppermute | solution.py:163
  24.1 0.0 collective-permute-start.4
  24.1 1.7 %collective-permute-start.5 = (bf16[17,16,128]{2,1,0:T(8,128)(2,1)}, bf16[17,16,128]{2,1,0:T(8,128)(2,1)S(1)}, u32[]{:S(2)}, u32[]{:S(2)}) collective-permute-start(bf16[17,16,128]{2,1,0:T(8,128)(2,1)} %shard_map.92.refs_0_), channel_id=1, source_target_pairs={{0,2},{2,0},{4,6},{6,4},{1,3},{3,1},{5,7},{7,5},{8,10},{10,8},{12,... | collective-permute-start | bytes 208904 | tf_op jit(solution)/shard_map/ppermute | solution.py:163
  25.8 0.0 copy-done.7
  25.8 0.1 concatenate.11
  25.9 2.6 %collective-permute-done.3.refs_1_ = bf16[17,16,128]{2,1,0:T(8,128)(2,1)S(1)} collective-permute-done((bf16[17,16,128]{2,1,0:T(8,128)(2,1)}, bf16[17,16,128]{2,1,0:T(8,128)(2,1)S(1)}, u32[]{:S(2)}, u32[]{:S(2)}) %collective-permute-start.3) | collective-permute-done | bytes 69664 | tf_op jit(solution)/shard_map/ppermute | solution.py:163
  28.5 2.2 %collective-permute-done.4.refs_2_ = bf16[17,16,128]{2,1,0:T(8,128)(2,1)S(1)} collective-permute-done((bf16[17,16,128]{2,1,0:T(8,128)(2,1)}, bf16[17,16,128]{2,1,0:T(8,128)(2,1)S(1)}, u32[]{:S(2)}, u32[]{:S(2)}) %collective-permute-start.4) | collective-permute-done | bytes 69664 | tf_op jit(solution)/shard_map/ppermute | solution.py:163
  30.7 0.0 collective-permute-done.5.refs_3_
  30.7 0.7 %broadcast_in_dim.7.refs_4_ = f32[16,128]{1,0:T(8,128)} broadcast(f32[16]{0:T(128)S(1)} %concatenate.11), dimensions={0} | broadcast | bytes 8256 | tf_op jit(solution)/shard_map/broadcast_in_dim | solution.py:188
  31.3 0.0 copy-done.3
  31.3 0.0 copy-done.4
  31.3 0.0 copy-done.5
  31.3 3.1 %shard_map.93 = (bf16[16,1024]{1,0:T(8,128)(2,1)}, f32[16,512]{1,0:T(8,128)}) custom-call(s32[1]{0:T(128)} %bitcast.side_ref, bf16[17,16,128]{2,1,0:T(8,128)(2,1)} %shard_map.92.refs_0_, bf16[17,16,128]{2,1,0:T(8,128)(2,1)} %copy-done.3, bf16[17,16,128]{2,1,0:T(8,128)(2,1)} %copy-done.4, bf16[17,16,128]{2,1,0:T(8,128)(2,1)} %copy-done.5, ...), custom_call_target="tpu_custom_call" | custom-call | flops 16777216 | bytes 1048576 | tf_op jit(solution)/shard_map/pallas_call | solution.py:211
  34.5 0.0 collective-permute-start.6
  34.5 2.5 %shard_map.94 = f32[16,512]{1,0:T(8,128)} custom-call(s32[1]{0:T(128)} %bitcast.side_ref, bf16[16,1024]{1,0:T(8,128)(2,1)} %get-tuple-element.7.normed_ref, bf16[1024,1024]{1,0:T(8,128)(2,1)} %weights_ref.3), custom_call_target="tpu_custom_call" | custom-call | flops 16777216 | bytes 1048576 | tf_op jit(solution)/shard_map/pallas_call | solution.py:222
  37.0 0.0 collective-permute-done.6
  37.0 1.4 %add_convert_fusion = bf16[16,512]{1,0:T(8,128)(2,1)} fusion(f32[16,512]{1,0:T(8,128)} %shard_map.94, f32[16,512]{1,0:T(8,128)S(1)} %collective-permute-done.6), kind=kLoop, calls=%fused_computation | loop fusion | flops 16384 | bytes 81920 | tf_op jit(solution)/shard_map/convert_element_type | solution.py:225
  (10 shorter events, 0.0 us)
Async XLA Ops:
  0.0 8.3 %copy-start.6 = (s32[16]{0:T(128)S(1)}, s32[16]{0:T(128)}, u32[]{:S(2)}) copy-start(s32[16]{0:T(128)} %param.17) | copy-start | bytes 196
  0.0 25.8 %copy-start.7 = (f32[8]{0:T(128)S(1)}, f32[8]{0:T(128)}, u32[]{:S(2)}) copy-start(f32[8]{0:T(128)} %param.12) | copy-start | bytes 100
  2.7 8.1 %collective-permute-start = (f32[9,16,128]{2,1,0:T(8,128)}, f32[9,16,128]{2,1,0:T(8,128)S(1)}, u32[]{:S(2)}, u32[]{:S(2)}) collective-permute-start(f32[9,16,128]{2,1,0:T(8,128)} %shard_map.91.refs_0_), channel_id=1, source_target_pairs={{0,6},{2,4},{4,2},{6,0},{1,7},{3,5},{5,3},{7,1},{8,14},{10,12},{12... | collective-permute-start | bytes 221192 | tf_op jit(solution)/shard_map/ppermute | solution.py:163
  7.8 6.4 %collective-permute-start.1 = (f32[9,16,128]{2,1,0:T(8,128)}, f32[9,16,128]{2,1,0:T(8,128)S(1)}, u32[]{:S(2)}, u32[]{:S(2)}) collective-permute-start(f32[9,16,128]{2,1,0:T(8,128)} %shard_map.91.refs_0_), channel_id=1, source_target_pairs={{0,4},{2,6},{4,0},{6,2},{1,5},{3,7},{5,1},{7,3},{8,12},{10,14},{12... | collective-permute-start | bytes 221192 | tf_op jit(solution)/shard_map/ppermute | solution.py:163
  7.8 6.4 %collective-permute-start.2 = (f32[9,16,128]{2,1,0:T(8,128)}, f32[9,16,128]{2,1,0:T(8,128)S(1)}, u32[]{:S(2)}, u32[]{:S(2)}) collective-permute-start(f32[9,16,128]{2,1,0:T(8,128)} %shard_map.91.refs_0_), channel_id=1, source_target_pairs={{0,2},{2,0},{4,6},{6,4},{1,3},{3,1},{5,7},{7,5},{8,10},{10,8},{12,... | collective-permute-start | bytes 221192 | tf_op jit(solution)/shard_map/ppermute | solution.py:163
  10.7 3.5 %copy-start = (f32[9,16,128]{2,1,0:T(8,128)}, f32[9,16,128]{2,1,0:T(8,128)S(1)}, u32[]{:S(2)}) copy-start(f32[9,16,128]{2,1,0:T(8,128)S(1)} %collective-permute-done.refs_1_) | copy-start | bytes 221188
  14.2 0.6 %copy-start.1 = (f32[9,16,128]{2,1,0:T(8,128)}, f32[9,16,128]{2,1,0:T(8,128)S(1)}, u32[]{:S(2)}) copy-start(f32[9,16,128]{2,1,0:T(8,128)S(1)} %collective-permute-done.1.refs_2_) | copy-start | bytes 221188
  14.2 0.7 %copy-start.2 = (f32[9,16,128]{2,1,0:T(8,128)}, f32[9,16,128]{2,1,0:T(8,128)S(1)}, u32[]{:S(2)}) copy-start(f32[9,16,128]{2,1,0:T(8,128)S(1)} %collective-permute-done.2.refs_3_) | copy-start | bytes 221188
  21.4 7.0 %collective-permute-start.3 = (bf16[17,16,128]{2,1,0:T(8,128)(2,1)}, bf16[17,16,128]{2,1,0:T(8,128)(2,1)S(1)}, u32[]{:S(2)}, u32[]{:S(2)}) collective-permute-start(bf16[17,16,128]{2,1,0:T(8,128)(2,1)} %shard_map.92.refs_0_), channel_id=1, source_target_pairs={{0,6},{2,4},{4,2},{6,0},{1,7},{3,5},{5,3},{7,1},{8,14},{10,12},{12... | collective-permute-start | bytes 208904 | tf_op jit(solution)/shard_map/ppermute | solution.py:163
  24.1 6.6 %collective-permute-start.4 = (bf16[17,16,128]{2,1,0:T(8,128)(2,1)}, bf16[17,16,128]{2,1,0:T(8,128)(2,1)S(1)}, u32[]{:S(2)}, u32[]{:S(2)}) collective-permute-start(bf16[17,16,128]{2,1,0:T(8,128)(2,1)} %shard_map.92.refs_0_), channel_id=1, source_target_pairs={{0,4},{2,6},{4,0},{6,2},{1,5},{3,7},{5,1},{7,3},{8,12},{10,14},{12... | collective-permute-start | bytes 208904 | tf_op jit(solution)/shard_map/ppermute | solution.py:163
  24.1 6.6 %collective-permute-start.5 = (bf16[17,16,128]{2,1,0:T(8,128)(2,1)}, bf16[17,16,128]{2,1,0:T(8,128)(2,1)S(1)}, u32[]{:S(2)}, u32[]{:S(2)}) collective-permute-start(bf16[17,16,128]{2,1,0:T(8,128)(2,1)} %shard_map.92.refs_0_), channel_id=1, source_target_pairs={{0,2},{2,0},{4,6},{6,4},{1,3},{3,1},{5,7},{7,5},{8,10},{10,8},{12,... | collective-permute-start | bytes 208904 | tf_op jit(solution)/shard_map/ppermute | solution.py:163
  28.5 2.9 %copy-start.3 = (bf16[17,16,128]{2,1,0:T(8,128)(2,1)}, bf16[17,16,128]{2,1,0:T(8,128)(2,1)S(1)}, u32[]{:S(2)}) copy-start(bf16[17,16,128]{2,1,0:T(8,128)(2,1)S(1)} %collective-permute-done.3.refs_1_) | copy-start | bytes 208900
  30.7 0.7 %copy-start.4 = (bf16[17,16,128]{2,1,0:T(8,128)(2,1)}, bf16[17,16,128]{2,1,0:T(8,128)(2,1)S(1)}, u32[]{:S(2)}) copy-start(bf16[17,16,128]{2,1,0:T(8,128)(2,1)S(1)} %collective-permute-done.4.refs_2_) | copy-start | bytes 208900
  30.7 0.7 %copy-start.5 = (bf16[17,16,128]{2,1,0:T(8,128)(2,1)}, bf16[17,16,128]{2,1,0:T(8,128)(2,1)S(1)}, u32[]{:S(2)}) copy-start(bf16[17,16,128]{2,1,0:T(8,128)(2,1)S(1)} %collective-permute-done.5.refs_3_) | copy-start | bytes 208900
  34.5 2.5 %collective-permute-start.6 = (f32[16,512]{1,0:T(8,128)}, f32[16,512]{1,0:T(8,128)S(1)}, u32[]{:S(2)}, u32[]{:S(2)}) collective-permute-start(f32[16,512]{1,0:T(8,128)} %get-tuple-element.8), channel_id=1, source_target_pairs={{0,1},{1,0},{2,3},{3,2},{4,5},{5,4},{6,7},{7,6},{8,9},{9,8},{10,11... | collective-permute-start | bytes 98312 | tf_op jit(solution)/shard_map/ppermute | solution.py:221

commit v2 on v1

--- a/solution.py
+++ b/solution.py
@@ -16,8 +16,11 @@
 MASKED = -1e30
 F32 = jnp.float32
 BF16 = jnp.bfloat16
+GRANT = 16 << 20
+CHUNKS = 4
 VMEM = pl.BlockSpec(memory_space=pltpu.VMEM)
 SMEM = pl.BlockSpec(memory_space=pltpu.SMEM)
+HBM = pl.BlockSpec(memory_space=pltpu.HBM)
 
 
 def lane_index(shape):
@@ -31,15 +34,69 @@
     return high, middle, (rest - middle).astype(BF16).astype(F32)
 
 
-def project_kernel(tokens_ref, gain_ref, weights_ref, out_ref):
+def project_kernel(tokens_hbm, gain_hbm, weights_hbm, out_ref, tokens_ref, gain_ref, weights_ref, done):
     heads = out_ref.shape[0] - 1
+    features = weights_ref.shape[0]
+    rows = features // CHUNKS
+    copies = [
+        pltpu.make_async_copy(tokens_hbm, tokens_ref, done.at[CHUNKS]),
+        pltpu.make_async_copy(gain_hbm, gain_ref, done.at[CHUNKS + 1]),
+    ]
+    for chunk in range(CHUNKS):
+        here = pl.ds(chunk * rows, rows)
+        copies.append(pltpu.make_async_copy(weights_hbm.at[here], weights_ref.at[here], done.at[chunk]))
+    for copy in copies:
+        copy.start()
+    copies[0].wait()
+    copies[1].wait()
     widened = tokens_ref[...].astype(F32)
     squares = jnp.sum(widened * widened, -1, keepdims=True)
     scaled = (widened * gain_ref[...]).astype(BF16)
-    part = jnp.dot(scaled, weights_ref[...], preferred_element_type=F32)
+    part = None
+    for chunk in range(CHUNKS):
+        here = slice(chunk * rows, (chunk + 1) * rows)
+        copies[2 + chunk].wait()
+        product = jnp.dot(scaled[:, here], weights_ref[here], preferred_element_type=F32)
+        part = product if part is None else part + product
     for head in range(heads):
         out_ref[head] = part[:, head * LANES : (head + 1) * LANES]
     out_ref[heads] = jnp.broadcast_to(squares, out_ref.shape[1:])
+
+
+def stage(sources, targets, done, meanwhile=None):
+    copies = [
+        pltpu.make_async_copy(source, target, done.at[i])
+        for i, (source, target) in enumerate(zip(sources, targets))
+    ]
+    for copy in copies:
+        copy.start()
+    if meanwhile is not None:
+        meanwhile()
+    for copy in copies:
+        copy.wait()
+
+
+def stage_cache_kernel(lengths_ref, first_ref, keys_hbm, values_hbm, limits_ref, keys_ref, values_ref, done):
+    def limits():
+        row = lax.broadcasted_iota(jnp.int32, limits_ref.shape, 0)
+        value = jnp.zeros(limits_ref.shape, jnp.int32)
+        for seq in range(limits_ref.shape[0]):
+            value = jnp.where(row == seq, lengths_ref[seq] - first_ref[0], value)
+        limits_ref[...] = value
+
+    stage((keys_hbm, values_hbm), (keys_ref, values_ref), done, limits)
+
+
+def stage_output_kernel(lambda_ref, weights_hbm, signs_ref, weights_ref, done):
+    def signs():
+        heads = signs_ref.shape[0] // 2
+        row = lax.broadcasted_iota(jnp.int32, signs_ref.shape, 0)
+        value = jnp.ones(signs_ref.shape, F32)
+        for head in range(heads):
+            value = jnp.where(row == heads + head, -lambda_ref[head], value)
+        signs_ref[...] = value
+
+    stage((weights_hbm,), (weights_ref,), done, signs)
 
 
 def attend_kernel(width, count, limits_ref, *refs):
@@ -77,7 +134,7 @@
             left, keys_ref[seq], (((1,), (1,)), ((), ())), preferred_element_type=F32
         )
         scores = products[:rows] + (products[rows : 2 * rows] + products[2 * rows :])
-        valid = places < limits_ref[seq]
+        valid = places < limits_ref[seq : seq + 1, :1]
         masked = jnp.where(valid, scores, MASKED)
         top = jnp.max(masked, -1, keepdims=True)
         weights = jnp.where(valid, jnp.exp(masked - top), 0.0)
@@ -151,8 +208,17 @@
         in_specs=in_specs,
         out_specs=out_specs,
         scratch_shapes=scratch,
+        compiler_params=pltpu.CompilerParams(vmem_limit_bytes=GRANT),
         cost_estimate=pl.CostEstimate(flops=flops, bytes_accessed=1 << 20, transcendentals=0),
     )
+
+
+def in_hbm(*arrays):
+    return tuple(pltpu.with_memory_space_constraint(x, pltpu.HBM) for x in arrays)
+
+
+def like(*arrays):
+    return tuple(jax.ShapeDtypeStruct(x.shape, x.dtype) for x in arrays)
 
 
 def exchanged(x, axis):
@@ -183,28 +249,45 @@
     positions = rotated_key_cache.shape[1]
     count = lax.axis_size("kv")
     cosine, sine = tables(lengths, LANES // HEAD_FEATURES)
-    limits = lengths - lax.axis_index("kv").astype(jnp.int32) * positions
+    first = (lax.axis_index("kv").astype(jnp.int32) * positions).reshape(1)
     side = lax.axis_index("tp").astype(jnp.int32).reshape(1)
-    signs = jnp.broadcast_to(
-        jnp.concatenate([jnp.ones_like(lambda_head), -lambda_head])[:, None], (2 * heads, LANES)
-    )
 
     partial = call(
         project_kernel,
         jax.ShapeDtypeStruct((heads + 1, seqs, LANES), F32),
-        [VMEM] * 3,
+        [HBM] * 3,
+        [
+            pltpu.VMEM((seqs, features), BF16),
+            pltpu.VMEM((1, features), F32),
+            pltpu.VMEM(w_query.shape, BF16),
+            pltpu.SemaphoreType.DMA((CHUNKS + 2,)),
+        ],
         flops=2 * seqs * features * heads * LANES,
-    )(tokens, norm_gain[None, :], w_query)
+    )(*in_hbm(tokens, norm_gain[None, :], w_query))
     queries = exchanged(partial, "kv")
+    limits, keys, values = call(
+        stage_cache_kernel,
+        (jax.ShapeDtypeStruct((seqs, LANES), jnp.int32), *like(rotated_key_cache, value_cache)),
+        [SMEM, SMEM, HBM, HBM],
+        [pltpu.SemaphoreType.DMA((2,))],
+        flops=1 << 20,
+    )(lengths, first, *in_hbm(rotated_key_cache, value_cache))
 
     blocks = call(
         functools.partial(attend_kernel, features * count, count),
         jax.ShapeDtypeStruct((seqs + 1, 2 * heads, LANES), BF16),
-        [SMEM] + [VMEM] * (count + 4),
+        [VMEM] * (count + 5),
         [pltpu.VMEM((seqs, heads, LANES), F32)],
         flops=8 * seqs * heads * positions * LANES,
-    )(limits, *queries, cosine, sine, rotated_key_cache, value_cache)
+    )(limits, *queries, cosine, sine, keys, values)
     gathered = exchanged(blocks, "kv")
+    signs, weights = call(
+        stage_output_kernel,
+        (jax.ShapeDtypeStruct((2 * heads, LANES), F32), *like(w_out)),
+        [SMEM, HBM],
+        [pltpu.SemaphoreType.DMA((1,))],
+        flops=1 << 20,
+    )(lambda_head, *in_hbm(w_out))
 
     columns = w_out.shape[1] // 2
     flops = 2 * seqs * heads * VALUE_DIM * columns
@@ -217,11 +300,11 @@
         [SMEM] + [VMEM] * (count + 3),
         [pltpu.VMEM((seqs, heads, LANES), F32)],
         flops=flops,
-    )(side, *gathered, signs, head_gain[None, :], w_out)
+    )(side, *gathered, signs, head_gain[None, :], weights)
     received = lax.ppermute(sent, "tp", [(0, 1), (1, 0)])
     own = call(
         own_kernel, jax.ShapeDtypeStruct((seqs, columns), F32), [SMEM, VMEM, VMEM], flops=flops
-    )(side, normed, w_out)
+    )(side, normed, weights)
     return (own + received).astype(BF16)
 
 

time: 38.6 us -> 29.8 us (0.77)
  Pallas kernels: 14.8 us -> 11.3 us
  waiting for transfers between devices: 9.29 us -> 7.25 us
  other arithmetic: 2.71 us -> 0.83 us
  local copies, waits for them, and re-layouts: 1.42 us -> 0.01 us
    pallas_call x0 -> x2, Pallas kernels: none -> 4.24 us  [the longest x1 2.14 us: near_device(): call(stage_output_kernel, (jax.ShapeDtypeStruct((2 * heads, LANES), F32),...]
    ppermute x6, waiting for transfers between devices: 9.28 us -> 6.29 us  [exchanged(): received.append(lax.ppermute(x, axis, pairs))]
    pallas_call x1, Pallas kernels: 3.13 us -> 0.74 us  [near_device(): call(functools.partial(finish_kernel, count), (jax.ShapeDtypeStruct((seqs...]
    pallas_call x1, Pallas kernels: 6.55 us -> 4.27 us  [near_device(): call(functools.partial(attend_kernel, features * count, count), jax.Shape...]
    pallas_call x1, Pallas kernels: 2.48 us -> 0.25 us  [near_device(): call(own_kernel, jax.ShapeDtypeStruct((seqs, columns), F32), [SMEM, VMEM,...]
    ppermute x1, waiting for transfers between devices: 0.01 us -> 0.96 us  [near_device(): received = lax.ppermute(sent, 'tp', [(0, 1), (1, 0)])]
    pallas_call x1, Pallas kernels: 2.69 us -> 1.8 us  [near_device(): call(project_kernel, jax.ShapeDtypeStruct((heads + 1, seqs, LANES), F32),...]
    convert_element_type x1, other arithmetic: 1.37 us -> 0.61 us  [near_device(): return (own + received).astype(BF16)]
  transfers between devices with their start and end apart: 7 -> 7, of which waited for: 4 -> 5; matrix products, arithmetic and copies ran while one was open for 4% -> 1% of each run, Pallas kernels for 6% -> 15%
where the time goes in v2:
time: 29.8 us; the launch traced here: 29.6 us
  Pallas kernels  11.3 us (38%)
  starting transfers between devices  10.1 us (34%)
  waiting for transfers between devices  7.25 us (24%)
  other arithmetic  0.83 us (3%)
    ppermute x6, starting transfers between devices, exchanged(): received.append(lax.ppermute(x, axis, pairs))  10.1 us
    ppermute x6, waiting for transfers between devices, exchanged(): received.append(lax.ppermute(x, axis, pairs))  6.29 us
    pallas_call x1, Pallas kernels, near_device(): call(functools.partial(attend_kernel, features * count, count), jax.Shape...  4.27 us
    pallas_call x1, Pallas kernels, near_device(): call(stage_output_kernel, (jax.ShapeDtypeStruct((2 * heads, LANES), F32),...  2.14 us
    pallas_call x1, Pallas kernels, near_device(): call(stage_cache_kernel, (jax.ShapeDtypeStruct((seqs, LANES), jnp.int32),...  2.1 us
    pallas_call x1, Pallas kernels, near_device(): call(project_kernel, jax.ShapeDtypeStruct((heads + 1, seqs, LANES), F32),...  1.8 us
    ppermute x1, waiting for transfers between devices, near_device(): received = lax.ppermute(sent, 'tp', [(0, 1), (1, 0)])  0.96 us
    pallas_call x1, Pallas kernels, near_device(): call(functools.partial(finish_kernel, count), (jax.ShapeDtypeStruct((seqs...  0.74 us
  transfers between devices with their start and end apart: 7, of which 5 were waited for; matrix products, arithmetic and copies ran while one was open for 1% of the time, Pallas kernels for 15%

profile of v2, /device:TPU:0, one launch (start us, length us, event | category | flops | bytes accessed | tf_op | source)
XLA Modules:
  0.0 29.6 jit_solution(3340075164721991771)
XLA Ops:
  0.0 0.0 copy-start.2
  0.0 1.8 %shard_map.92.refs_0_ = f32[9,16,128]{2,1,0:T(8,128)S(1)} custom-call(bf16[16,1024]{1,0:T(8,128)(2,1)} %tokens_hbm.1, f32[1,1024]{1,0:T(1,128)} %bitcast.5, bf16[1024,1024]{1,0:T(8,128)(2,1)} %weights_hbm.2), custom_call_target="tpu_custom_call" | custom-call | flops 33554432 | bytes 1048576 | tf_op jit(solution)/shard_map/pallas_call | solution.py:255
  1.8 3.1 %collective-permute-start.2 = (f32[9,16,128]{2,1,0:T(8,128)S(1)}, f32[9,16,128]{2,1,0:T(8,128)S(1)}, u32[]{:S(2)}, u32[]{:S(2)}) collective-permute-start(f32[9,16,128]{2,1,0:T(8,128)S(1)} %shard_map.92.refs_0_), channel_id=1, source_target_pairs={{0,2},{2,0},{4,6},{6,4},{1,3},{3,1},{5,7},{7,5},{8,10},{10,8},{12,... | collective-permute-start | bytes 221192 | tf_op jit(solution)/shard_map/ppermute | solution.py:229
  4.9 2.6 %collective-permute-start.1 = (f32[9,16,128]{2,1,0:T(8,128)S(1)}, f32[9,16,128]{2,1,0:T(8,128)S(1)}, u32[]{:S(2)}, u32[]{:S(2)}) collective-permute-start(f32[9,16,128]{2,1,0:T(8,128)S(1)} %shard_map.92.refs_0_), channel_id=1, source_target_pairs={{0,4},{2,6},{4,0},{6,2},{1,5},{3,7},{5,1},{7,3},{8,12},{10,14},{12... | collective-permute-start | bytes 221192 | tf_op jit(solution)/shard_map/ppermute | solution.py:229
  7.5 0.0 collective-permute-start
  7.5 0.0 copy-done.2
  7.6 0.1 fusion
  7.7 0.0 copy-start
  7.7 2.1 %shard_map.91 = (s32[16,128]{1,0:T(8,128)S(1)}, bf16[16,256,128]{2,1,0:T(8,128)(2,1)S(1)}, bf16[16,256,128]{2,1,0:T(8,128)(2,1)S(1)}) custom-call(s32[16]{0:T(128)S(1)} %copy-done.2, s32[1]{0:T(128)} %bitcast.1.first_ref, bf16[16,256,128]{2,1,0:T(8,128)(2,1)} %keys_hbm.1, bf16[16,256,128]{2,1,0:T(8,128)(2,1)} %values_hbm.1), custom_call_target="tpu_custom_call" | custom-call | flops 1048576 | bytes 1048576 | tf_op jit(solution)/shard_map/pallas_call | solution.py:268
  9.8 0.1 pad_maximum_fusion
  9.9 0.0 collective-permute-done.2.refs_3_
  9.9 2.8 %collective-permute-done.1.refs_2_ = f32[9,16,128]{2,1,0:T(8,128)S(1)} collective-permute-done((f32[9,16,128]{2,1,0:T(8,128)S(1)}, f32[9,16,128]{2,1,0:T(8,128)S(1)}, u32[]{:S(2)}, u32[]{:S(2)}) %collective-permute-start.1) | collective-permute-done | bytes 73760 | tf_op jit(solution)/shard_map/ppermute | solution.py:229
  12.7 1.1 %collective-permute-done.refs_1_ = f32[9,16,128]{2,1,0:T(8,128)S(1)} collective-permute-done((f32[9,16,128]{2,1,0:T(8,128)S(1)}, f32[9,16,128]{2,1,0:T(8,128)S(1)}, u32[]{:S(2)}, u32[]{:S(2)}) %collective-permute-start) | collective-permute-done | bytes 73760 | tf_op jit(solution)/shard_map/ppermute | solution.py:229
  13.8 0.0 copy-start.1
  13.8 4.3 %shard_map.93.refs_0_ = bf16[17,16,128]{2,1,0:T(8,128)(2,1)S(1)} custom-call(s32[16,128]{1,0:T(8,128)S(1)} %get-tuple-element.12.limits_ref, f32[9,16,128]{2,1,0:T(8,128)S(1)} %shard_map.92.refs_0_, f32[9,16,128]{2,1,0:T(8,128)S(1)} %collective-permute-done.refs_1_, f32[9,16,128]{2,1,0:T(8,128)S(1)} %collective-permute-done.1.refs_2_, ...), custom_call_target="tpu_custom_call" | custom-call | flops 33554432 | bytes 1048576 | tf_op jit(solution)/shard_map/pallas_call | solution.py:276
  18.0 1.1 %collective-permute-start.5 = (bf16[17,16,128]{2,1,0:T(8,128)(2,1)S(1)}, bf16[17,16,128]{2,1,0:T(8,128)(2,1)S(1)}, u32[]{:S(2)}, u32[]{:S(2)}) collective-permute-start(bf16[17,16,128]{2,1,0:T(8,128)(2,1)S(1)} %shard_map.93.refs_0_), channel_id=1, source_target_pairs={{0,2},{2,0},{4,6},{6,4},{1,3},{3,1},{5,7},{7,5},{8,10},{10,8},{12,... | collective-permute-start | bytes 208904 | tf_op jit(solution)/shard_map/ppermute | solution.py:229
  19.2 1.7 %collective-permute-start.4 = (bf16[17,16,128]{2,1,0:T(8,128)(2,1)S(1)}, bf16[17,16,128]{2,1,0:T(8,128)(2,1)S(1)}, u32[]{:S(2)}, u32[]{:S(2)}) collective-permute-start(bf16[17,16,128]{2,1,0:T(8,128)(2,1)S(1)} %shard_map.93.refs_0_), channel_id=1, source_target_pairs={{0,4},{2,6},{4,0},{6,2},{1,5},{3,7},{5,1},{7,3},{8,12},{10,14},{12... | collective-permute-start | bytes 208904 | tf_op jit(solution)/shard_map/ppermute | solution.py:229
  20.8 1.6 %collective-permute-start.3 = (bf16[17,16,128]{2,1,0:T(8,128)(2,1)S(1)}, bf16[17,16,128]{2,1,0:T(8,128)(2,1)S(1)}, u32[]{:S(2)}, u32[]{:S(2)}) collective-permute-start(bf16[17,16,128]{2,1,0:T(8,128)(2,1)S(1)} %shard_map.93.refs_0_), channel_id=1, source_target_pairs={{0,6},{2,4},{4,2},{6,0},{1,7},{3,5},{5,3},{7,1},{8,14},{10,12},{12... | collective-permute-start | bytes 208904 | tf_op jit(solution)/shard_map/ppermute | solution.py:229
  22.5 0.0 copy-done
  22.5 2.1 %shard_map.94 = (f32[16,128]{1,0:T(8,128)S(1)}, bf16[1024,1024]{1,0:T(8,128)(2,1)S(1)}) custom-call(f32[8]{0:T(128)S(1)} %copy-done, bf16[1024,1024]{1,0:T(8,128)(2,1)} %weights_hbm.3), custom_call_target="tpu_custom_call" | custom-call | flops 1048576 | bytes 1048576 | tf_op jit(solution)/shard_map/pallas_call | solution.py:284
  24.6 0.0 collective-permute-done.5.refs_3_
  24.6 0.9 %collective-permute-done.4.refs_2_ = bf16[17,16,128]{2,1,0:T(8,128)(2,1)S(1)} collective-permute-done((bf16[17,16,128]{2,1,0:T(8,128)(2,1)S(1)}, bf16[17,16,128]{2,1,0:T(8,128)(2,1)S(1)}, u32[]{:S(2)}, u32[]{:S(2)}) %collective-permute-start.4) | collective-permute-done | bytes 69664 | tf_op jit(solution)/shard_map/ppermute | solution.py:229
  25.5 1.5 %collective-permute-done.3.refs_1_ = bf16[17,16,128]{2,1,0:T(8,128)(2,1)S(1)} collective-permute-done((bf16[17,16,128]{2,1,0:T(8,128)(2,1)S(1)}, bf16[17,16,128]{2,1,0:T(8,128)(2,1)S(1)}, u32[]{:S(2)}, u32[]{:S(2)}) %collective-permute-start.3) | collective-permute-done | bytes 69664 | tf_op jit(solution)/shard_map/ppermute | solution.py:229
  27.0 0.0 copy-done.1
  27.0 0.7 %shard_map.95 = (bf16[16,1024]{1,0:T(8,128)(2,1)S(1)}, f32[16,512]{1,0:T(8,128)S(1)}) custom-call(s32[1]{0:T(128)} %bitcast.side_ref, bf16[17,16,128]{2,1,0:T(8,128)(2,1)S(1)} %shard_map.93.refs_0_, bf16[17,16,128]{2,1,0:T(8,128)(2,1)S(1)} %collective-permute-done.3.refs_1_, bf16[17,16,128]{2,1,0:T(8,128)(2,1)S(1)} %collective-permute-done.4.refs_2_, ...), custom_call_target="tpu_custom_call" | custom-call | flops 16777216 | bytes 1048576 | tf_op jit(solution)/shard_map/pallas_call | solution.py:294
  27.8 0.0 collective-permute-start.6
  27.8 0.2 shard_map.96
  28.0 1.0 %collective-permute-done.6 = f32[16,512]{1,0:T(8,128)S(1)} collective-permute-done((f32[16,512]{1,0:T(8,128)S(1)}, f32[16,512]{1,0:T(8,128)S(1)}, u32[]{:S(2)}, u32[]{:S(2)}) %collective-permute-start.6) | collective-permute-done | bytes 32800 | tf_op jit(solution)/shard_map/ppermute | solution.py:304
  29.0 0.6 %add_convert_fusion = bf16[16,512]{1,0:T(8,128)(2,1)} fusion(f32[16,512]{1,0:T(8,128)S(1)} %shard_map.96, f32[16,512]{1,0:T(8,128)S(1)} %collective-permute-done.6), kind=kLoop, calls=%fused_computation | loop fusion | flops 16384 | bytes 81920 | tf_op jit(solution)/shard_map/convert_element_type | solution.py:308
  (2 shorter events, 0.0 us)
Async XLA Ops:
  0.0 7.5 %copy-start.2 = (s32[16]{0:T(128)S(1)}, s32[16]{0:T(128)}, u32[]{:S(2)}) copy-start(s32[16]{0:T(128)} %lengths_ref.1) | copy-start | bytes 196
  1.8 8.1 %collective-permute-start.2 = (f32[9,16,128]{2,1,0:T(8,128)S(1)}, f32[9,16,128]{2,1,0:T(8,128)S(1)}, u32[]{:S(2)}, u32[]{:S(2)}) collective-permute-start(f32[9,16,128]{2,1,0:T(8,128)S(1)} %shard_map.92.refs_0_), channel_id=1, source_target_pairs={{0,2},{2,0},{4,6},{6,4},{1,3},{3,1},{5,7},{7,5},{8,10},{10,8},{12,... | collective-permute-start | bytes 221192 | tf_op jit(solution)/shard_map/ppermute | solution.py:229
  4.9 7.8 %collective-permute-start.1 = (f32[9,16,128]{2,1,0:T(8,128)S(1)}, f32[9,16,128]{2,1,0:T(8,128)S(1)}, u32[]{:S(2)}, u32[]{:S(2)}) collective-permute-start(f32[9,16,128]{2,1,0:T(8,128)S(1)} %shard_map.92.refs_0_), channel_id=1, source_target_pairs={{0,4},{2,6},{4,0},{6,2},{1,5},{3,7},{5,1},{7,3},{8,12},{10,14},{12... | collective-permute-start | bytes 221192 | tf_op jit(solution)/shard_map/ppermute | solution.py:229
  7.5 6.3 %collective-permute-start = (f32[9,16,128]{2,1,0:T(8,128)S(1)}, f32[9,16,128]{2,1,0:T(8,128)S(1)}, u32[]{:S(2)}, u32[]{:S(2)}) collective-permute-start(f32[9,16,128]{2,1,0:T(8,128)S(1)} %shard_map.92.refs_0_), channel_id=1, source_target_pairs={{0,6},{2,4},{4,2},{6,0},{1,7},{3,5},{5,3},{7,1},{8,14},{10,12},{12... | collective-permute-start | bytes 221192 | tf_op jit(solution)/shard_map/ppermute | solution.py:229
  7.7 14.8 %copy-start = (f32[8]{0:T(128)S(1)}, f32[8]{0:T(128)}, u32[]{:S(2)}) copy-start(f32[8]{0:T(128)} %lambda_ref.1) | copy-start | bytes 100
  13.8 13.3 %copy-start.1 = (f32[128]{0:T(128)S(1)}, f32[128]{0:T(128)}, u32[]{:S(2)}) copy-start(f32[128]{0:T(128)} %param.13) | copy-start | bytes 1540
  18.0 6.6 %collective-permute-start.5 = (bf16[17,16,128]{2,1,0:T(8,128)(2,1)S(1)}, bf16[17,16,128]{2,1,0:T(8,128)(2,1)S(1)}, u32[]{:S(2)}, u32[]{:S(2)}) collective-permute-start(bf16[17,16,128]{2,1,0:T(8,128)(2,1)S(1)} %shard_map.93.refs_0_), channel_id=1, source_target_pairs={{0,2},{2,0},{4,6},{6,4},{1,3},{3,1},{5,7},{7,5},{8,10},{10,8},{12,... | collective-permute-start | bytes 208904 | tf_op jit(solution)/shard_map/ppermute | solution.py:229
  19.2 6.4 %collective-permute-start.4 = (bf16[17,16,128]{2,1,0:T(8,128)(2,1)S(1)}, bf16[17,16,128]{2,1,0:T(8,128)(2,1)S(1)}, u32[]{:S(2)}, u32[]{:S(2)}) collective-permute-start(bf16[17,16,128]{2,1,0:T(8,128)(2,1)S(1)} %shard_map.93.refs_0_), channel_id=1, source_target_pairs={{0,4},{2,6},{4,0},{6,2},{1,5},{3,7},{5,1},{7,3},{8,12},{10,14},{12... | collective-permute-start | bytes 208904 | tf_op jit(solution)/shard_map/ppermute | solution.py:229
  20.8 6.2 %collective-permute-start.3 = (bf16[17,16,128]{2,1,0:T(8,128)(2,1)S(1)}, bf16[17,16,128]{2,1,0:T(8,128)(2,1)S(1)}, u32[]{:S(2)}, u32[]{:S(2)}) collective-permute-start(bf16[17,16,128]{2,1,0:T(8,128)(2,1)S(1)} %shard_map.93.refs_0_), channel_id=1, source_target_pairs={{0,6},{2,4},{4,2},{6,0},{1,7},{3,5},{5,3},{7,1},{8,14},{10,12},{12... | collective-permute-start | bytes 208904 | tf_op jit(solution)/shard_map/ppermute | solution.py:229
  27.8 1.2 %collective-permute-start.6 = (f32[16,512]{1,0:T(8,128)S(1)}, f32[16,512]{1,0:T(8,128)S(1)}, u32[]{:S(2)}, u32[]{:S(2)}) collective-permute-start(f32[16,512]{1,0:T(8,128)S(1)} %get-tuple-element.18), channel_id=1, source_target_pairs={{0,1},{1,0},{2,3},{3,2},{4,5},{5,4},{6,7},{7,6},{8,9},{9,8},{10,11... | collective-permute-start | bytes 98312 | tf_op jit(solution)/shard_map/ppermute | solution.py:304

commit v3 on v2

--- a/solution.py
+++ b/solution.py
@@ -125,6 +125,7 @@
     places = lane_index((rows, positions))
     maxima = jnp.zeros((rows, LANES), F32)
     totals = jnp.zeros((rows, LANES), F32)
+    scores = []
     for seq in range(seqs):
         pieces = split3(query_ref[seq])
         left = jnp.concatenate(
@@ -133,16 +134,21 @@
         products = lax.dot_general(
             left, keys_ref[seq], (((1,), (1,)), ((), ())), preferred_element_type=F32
         )
-        scores = products[:rows] + (products[rows : 2 * rows] + products[2 * rows :])
+        scores.append(products[:rows] + (products[rows : 2 * rows] + products[2 * rows :]))
+    weights = []
+    for seq in range(seqs):
         valid = places < limits_ref[seq : seq + 1, :1]
-        masked = jnp.where(valid, scores, MASKED)
+        masked = jnp.where(valid, scores[seq], MASKED)
         top = jnp.max(masked, -1, keepdims=True)
-        weights = jnp.where(valid, jnp.exp(masked - top), 0.0)
+        weight = jnp.where(valid, jnp.exp(masked - top), 0.0)
         maxima = jnp.where(lanes == seq, top, maxima)
-        totals = jnp.where(lanes == seq, jnp.sum(weights, -1, keepdims=True), totals)
-        out_ref[seq] = jnp.dot(
-            weights.astype(BF16), values_ref[seq], preferred_element_type=F32
-        ).astype(BF16)
+        totals = jnp.where(lanes == seq, jnp.sum(weight, -1, keepdims=True), totals)
+        weights.append(weight.astype(BF16))
+    numerators = [
+        jnp.dot(weights[seq], values_ref[seq], preferred_element_type=F32) for seq in range(seqs)
+    ]
+    for seq in range(seqs):
+        out_ref[seq] = numerators[seq].astype(BF16)
     packed = jnp.zeros((rows, LANES), F32)
     for place, piece in enumerate(split3(maxima) + split3(totals)):
         inside = (lanes >= place * seqs) & (lanes < (place + 1) * seqs)

time: 29.8 us -> 26.3 us (0.88)
  Pallas kernels: 11.3 us -> 7.8 us
    pallas_call x1, Pallas kernels: 4.27 us -> 0.77 us  [near_device(): call(functools.partial(attend_kernel, features * count, count), jax.Shape...]
  transfers between devices with their start and end apart: 7 -> 7, of which waited for: 5 -> 5; matrix products, arithmetic and copies ran while one was open for 1% -> 1% of each run, Pallas kernels for 15% -> 17%
where the time goes in v3:
time: 26.3 us; the launch traced here: 26.1 us
  starting transfers between devices  10.1 us (38%)
  Pallas kernels  7.8 us (30%)
  waiting for transfers between devices  7.26 us (28%)
  other arithmetic  0.83 us (3%)
    ppermute x6, starting transfers between devices, exchanged(): received.append(lax.ppermute(x, axis, pairs))  10.1 us
    ppermute x6, waiting for transfers between devices, exchanged(): received.append(lax.ppermute(x, axis, pairs))  6.29 us
    pallas_call x1, Pallas kernels, near_device(): call(stage_output_kernel, (jax.ShapeDtypeStruct((2 * heads, LANES), F32),...  2.14 us
    pallas_call x1, Pallas kernels, near_device(): call(stage_cache_kernel, (jax.ShapeDtypeStruct((seqs, LANES), jnp.int32),...  2.1 us
    pallas_call x1, Pallas kernels, near_device(): call(project_kernel, jax.ShapeDtypeStruct((heads + 1, seqs, LANES), F32),...  1.8 us
    ppermute x1, waiting for transfers between devices, near_device(): received = lax.ppermute(sent, 'tp', [(0, 1), (1, 0)])  0.96 us
    pallas_call x1, Pallas kernels, near_device(): call(functools.partial(attend_kernel, features * count, count), jax.Shape...  0.77 us
    pallas_call x1, Pallas kernels, near_device(): call(functools.partial(finish_kernel, count), (jax.ShapeDtypeStruct((seqs...  0.74 us
  transfers between devices with their start and end apart: 7, of which 5 were waited for; matrix products, arithmetic and copies ran while one was open for 1% of the time, Pallas kernels for 17%

profile of v3, /device:TPU:0, one launch (start us, length us, event | category | flops | bytes accessed | tf_op | source)
XLA Modules:
  0.0 26.1 jit_solution(5899191427733024784)
XLA Ops:
  0.0 0.0 copy-start.2
  0.0 1.8 %shard_map.92.refs_0_ = f32[9,16,128]{2,1,0:T(8,128)S(1)} custom-call(bf16[16,1024]{1,0:T(8,128)(2,1)} %tokens_hbm.1, f32[1,1024]{1,0:T(1,128)} %bitcast.5, bf16[1024,1024]{1,0:T(8,128)(2,1)} %weights_hbm.2), custom_call_target="tpu_custom_call" | custom-call | flops 33554432 | bytes 1048576 | tf_op jit(solution)/shard_map/pallas_call | solution.py:261
  1.8 3.1 %collective-permute-start.2 = (f32[9,16,128]{2,1,0:T(8,128)S(1)}, f32[9,16,128]{2,1,0:T(8,128)S(1)}, u32[]{:S(2)}, u32[]{:S(2)}) collective-permute-start(f32[9,16,128]{2,1,0:T(8,128)S(1)} %shard_map.92.refs_0_), channel_id=1, source_target_pairs={{0,2},{2,0},{4,6},{6,4},{1,3},{3,1},{5,7},{7,5},{8,10},{10,8},{12,... | collective-permute-start | bytes 221192 | tf_op jit(solution)/shard_map/ppermute | solution.py:235
  4.9 2.6 %collective-permute-start.1 = (f32[9,16,128]{2,1,0:T(8,128)S(1)}, f32[9,16,128]{2,1,0:T(8,128)S(1)}, u32[]{:S(2)}, u32[]{:S(2)}) collective-permute-start(f32[9,16,128]{2,1,0:T(8,128)S(1)} %shard_map.92.refs_0_), channel_id=1, source_target_pairs={{0,4},{2,6},{4,0},{6,2},{1,5},{3,7},{5,1},{7,3},{8,12},{10,14},{12... | collective-permute-start | bytes 221192 | tf_op jit(solution)/shard_map/ppermute | solution.py:235
  7.5 0.0 collective-permute-start
  7.5 0.0 copy-done.2
  7.6 0.1 fusion
  7.7 0.0 copy-start
  7.7 2.1 %shard_map.91 = (s32[16,128]{1,0:T(8,128)S(1)}, bf16[16,256,128]{2,1,0:T(8,128)(2,1)S(1)}, bf16[16,256,128]{2,1,0:T(8,128)(2,1)S(1)}) custom-call(s32[16]{0:T(128)S(1)} %copy-done.2, s32[1]{0:T(128)} %bitcast.1.first_ref, bf16[16,256,128]{2,1,0:T(8,128)(2,1)} %keys_hbm.1, bf16[16,256,128]{2,1,0:T(8,128)(2,1)} %values_hbm.1), custom_call_target="tpu_custom_call" | custom-call | flops 1048576 | bytes 1048576 | tf_op jit(solution)/shard_map/pallas_call | solution.py:274
  9.8 0.1 pad_maximum_fusion
  9.9 0.0 collective-permute-done.2.refs_3_
  9.9 2.8 %collective-permute-done.1.refs_2_ = f32[9,16,128]{2,1,0:T(8,128)S(1)} collective-permute-done((f32[9,16,128]{2,1,0:T(8,128)S(1)}, f32[9,16,128]{2,1,0:T(8,128)S(1)}, u32[]{:S(2)}, u32[]{:S(2)}) %collective-permute-start.1) | collective-permute-done | bytes 73760 | tf_op jit(solution)/shard_map/ppermute | solution.py:235
  12.7 1.1 %collective-permute-done.refs_1_ = f32[9,16,128]{2,1,0:T(8,128)S(1)} collective-permute-done((f32[9,16,128]{2,1,0:T(8,128)S(1)}, f32[9,16,128]{2,1,0:T(8,128)S(1)}, u32[]{:S(2)}, u32[]{:S(2)}) %collective-permute-start) | collective-permute-done | bytes 73760 | tf_op jit(solution)/shard_map/ppermute | solution.py:235
  13.8 0.0 copy-start.1
  13.8 0.8 %shard_map.93.refs_0_ = bf16[17,16,128]{2,1,0:T(8,128)(2,1)S(1)} custom-call(s32[16,128]{1,0:T(8,128)S(1)} %get-tuple-element.12.limits_ref, f32[9,16,128]{2,1,0:T(8,128)S(1)} %shard_map.92.refs_0_, f32[9,16,128]{2,1,0:T(8,128)S(1)} %collective-permute-done.refs_1_, f32[9,16,128]{2,1,0:T(8,128)S(1)} %collective-permute-done.1.refs_2_, ...), custom_call_target="tpu_custom_call" | custom-call | flops 33554432 | bytes 1048576 | tf_op jit(solution)/shard_map/pallas_call | solution.py:282
  14.5 1.1 %collective-permute-start.5 = (bf16[17,16,128]{2,1,0:T(8,128)(2,1)S(1)}, bf16[17,16,128]{2,1,0:T(8,128)(2,1)S(1)}, u32[]{:S(2)}, u32[]{:S(2)}) collective-permute-start(bf16[17,16,128]{2,1,0:T(8,128)(2,1)S(1)} %shard_map.93.refs_0_), channel_id=1, source_target_pairs={{0,2},{2,0},{4,6},{6,4},{1,3},{3,1},{5,7},{7,5},{8,10},{10,8},{12,... | collective-permute-start | bytes 208904 | tf_op jit(solution)/shard_map/ppermute | solution.py:235
  15.7 1.7 %collective-permute-start.4 = (bf16[17,16,128]{2,1,0:T(8,128)(2,1)S(1)}, bf16[17,16,128]{2,1,0:T(8,128)(2,1)S(1)}, u32[]{:S(2)}, u32[]{:S(2)}) collective-permute-start(bf16[17,16,128]{2,1,0:T(8,128)(2,1)S(1)} %shard_map.93.refs_0_), channel_id=1, source_target_pairs={{0,4},{2,6},{4,0},{6,2},{1,5},{3,7},{5,1},{7,3},{8,12},{10,14},{12... | collective-permute-start | bytes 208904 | tf_op jit(solution)/shard_map/ppermute | solution.py:235
  17.4 1.6 %collective-permute-start.3 = (bf16[17,16,128]{2,1,0:T(8,128)(2,1)S(1)}, bf16[17,16,128]{2,1,0:T(8,128)(2,1)S(1)}, u32[]{:S(2)}, u32[]{:S(2)}) collective-permute-start(bf16[17,16,128]{2,1,0:T(8,128)(2,1)S(1)} %shard_map.93.refs_0_), channel_id=1, source_target_pairs={{0,6},{2,4},{4,2},{6,0},{1,7},{3,5},{5,3},{7,1},{8,14},{10,12},{12... | collective-permute-start | bytes 208904 | tf_op jit(solution)/shard_map/ppermute | solution.py:235
  19.0 0.0 copy-done
  19.0 2.1 %shard_map.94 = (f32[16,128]{1,0:T(8,128)S(1)}, bf16[1024,1024]{1,0:T(8,128)(2,1)S(1)}) custom-call(f32[8]{0:T(128)S(1)} %copy-done, bf16[1024,1024]{1,0:T(8,128)(2,1)} %weights_hbm.3), custom_call_target="tpu_custom_call" | custom-call | flops 1048576 | bytes 1048576 | tf_op jit(solution)/shard_map/pallas_call | solution.py:290
  21.1 0.0 collective-permute-done.5.refs_3_
  21.1 0.9 %collective-permute-done.4.refs_2_ = bf16[17,16,128]{2,1,0:T(8,128)(2,1)S(1)} collective-permute-done((bf16[17,16,128]{2,1,0:T(8,128)(2,1)S(1)}, bf16[17,16,128]{2,1,0:T(8,128)(2,1)S(1)}, u32[]{:S(2)}, u32[]{:S(2)}) %collective-permute-start.4) | collective-permute-done | bytes 69664 | tf_op jit(solution)/shard_map/ppermute | solution.py:235
  22.0 1.5 %collective-permute-done.3.refs_1_ = bf16[17,16,128]{2,1,0:T(8,128)(2,1)S(1)} collective-permute-done((bf16[17,16,128]{2,1,0:T(8,128)(2,1)S(1)}, bf16[17,16,128]{2,1,0:T(8,128)(2,1)S(1)}, u32[]{:S(2)}, u32[]{:S(2)}) %collective-permute-start.3) | collective-permute-done | bytes 69664 | tf_op jit(solution)/shard_map/ppermute | solution.py:235
  23.5 0.0 copy-done.1
  23.5 0.7 %shard_map.95 = (bf16[16,1024]{1,0:T(8,128)(2,1)S(1)}, f32[16,512]{1,0:T(8,128)S(1)}) custom-call(s32[1]{0:T(128)} %bitcast.side_ref, bf16[17,16,128]{2,1,0:T(8,128)(2,1)S(1)} %shard_map.93.refs_0_, bf16[17,16,128]{2,1,0:T(8,128)(2,1)S(1)} %collective-permute-done.3.refs_1_, bf16[17,16,128]{2,1,0:T(8,128)(2,1)S(1)} %collective-permute-done.4.refs_2_, ...), custom_call_target="tpu_custom_call" | custom-call | flops 16777216 | bytes 1048576 | tf_op jit(solution)/shard_map/pallas_call | solution.py:300
  24.3 0.0 collective-permute-start.6
  24.3 0.2 shard_map.96
  24.5 1.0 %collective-permute-done.6 = f32[16,512]{1,0:T(8,128)S(1)} collective-permute-done((f32[16,512]{1,0:T(8,128)S(1)}, f32[16,512]{1,0:T(8,128)S(1)}, u32[]{:S(2)}, u32[]{:S(2)}) %collective-permute-start.6) | collective-permute-done | bytes 32800 | tf_op jit(solution)/shard_map/ppermute | solution.py:310
  25.5 0.6 %add_convert_fusion = bf16[16,512]{1,0:T(8,128)(2,1)} fusion(f32[16,512]{1,0:T(8,128)S(1)} %shard_map.96, f32[16,512]{1,0:T(8,128)S(1)} %collective-permute-done.6), kind=kLoop, calls=%fused_computation | loop fusion | flops 16384 | bytes 81920 | tf_op jit(solution)/shard_map/convert_element_type | solution.py:314
  (2 shorter events, 0.0 us)
Async XLA Ops:
  0.0 7.5 %copy-start.2 = (s32[16]{0:T(128)S(1)}, s32[16]{0:T(128)}, u32[]{:S(2)}) copy-start(s32[16]{0:T(128)} %lengths_ref.1) | copy-start | bytes 196
  1.8 8.1 %collective-permute-start.2 = (f32[9,16,128]{2,1,0:T(8,128)S(1)}, f32[9,16,128]{2,1,0:T(8,128)S(1)}, u32[]{:S(2)}, u32[]{:S(2)}) collective-permute-start(f32[9,16,128]{2,1,0:T(8,128)S(1)} %shard_map.92.refs_0_), channel_id=1, source_target_pairs={{0,2},{2,0},{4,6},{6,4},{1,3},{3,1},{5,7},{7,5},{8,10},{10,8},{12,... | collective-permute-start | bytes 221192 | tf_op jit(solution)/shard_map/ppermute | solution.py:235
  4.9 7.8 %collective-permute-start.1 = (f32[9,16,128]{2,1,0:T(8,128)S(1)}, f32[9,16,128]{2,1,0:T(8,128)S(1)}, u32[]{:S(2)}, u32[]{:S(2)}) collective-permute-start(f32[9,16,128]{2,1,0:T(8,128)S(1)} %shard_map.92.refs_0_), channel_id=1, source_target_pairs={{0,4},{2,6},{4,0},{6,2},{1,5},{3,7},{5,1},{7,3},{8,12},{10,14},{12... | collective-permute-start | bytes 221192 | tf_op jit(solution)/shard_map/ppermute | solution.py:235
  7.5 6.3 %collective-permute-start = (f32[9,16,128]{2,1,0:T(8,128)S(1)}, f32[9,16,128]{2,1,0:T(8,128)S(1)}, u32[]{:S(2)}, u32[]{:S(2)}) collective-permute-start(f32[9,16,128]{2,1,0:T(8,128)S(1)} %shard_map.92.refs_0_), channel_id=1, source_target_pairs={{0,6},{2,4},{4,2},{6,0},{1,7},{3,5},{5,3},{7,1},{8,14},{10,12},{12... | collective-permute-start | bytes 221192 | tf_op jit(solution)/shard_map/ppermute | solution.py:235
  7.7 11.3 %copy-start = (f32[8]{0:T(128)S(1)}, f32[8]{0:T(128)}, u32[]{:S(2)}) copy-start(f32[8]{0:T(128)} %lambda_ref.1) | copy-start | bytes 100
  13.8 9.8 %copy-start.1 = (f32[128]{0:T(128)S(1)}, f32[128]{0:T(128)}, u32[]{:S(2)}) copy-start(f32[128]{0:T(128)} %param.13) | copy-start | bytes 1540
  14.5 6.6 %collective-permute-start.5 = (bf16[17,16,128]{2,1,0:T(8,128)(2,1)S(1)}, bf16[17,16,128]{2,1,0:T(8,128)(2,1)S(1)}, u32[]{:S(2)}, u32[]{:S(2)}) collective-permute-start(bf16[17,16,128]{2,1,0:T(8,128)(2,1)S(1)} %shard_map.93.refs_0_), channel_id=1, source_target_pairs={{0,2},{2,0},{4,6},{6,4},{1,3},{3,1},{5,7},{7,5},{8,10},{10,8},{12,... | collective-permute-start | bytes 208904 | tf_op jit(solution)/shard_map/ppermute | solution.py:235
  15.7 6.4 %collective-permute-start.4 = (bf16[17,16,128]{2,1,0:T(8,128)(2,1)S(1)}, bf16[17,16,128]{2,1,0:T(8,128)(2,1)S(1)}, u32[]{:S(2)}, u32[]{:S(2)}) collective-permute-start(bf16[17,16,128]{2,1,0:T(8,128)(2,1)S(1)} %shard_map.93.refs_0_), channel_id=1, source_target_pairs={{0,4},{2,6},{4,0},{6,2},{1,5},{3,7},{5,1},{7,3},{8,12},{10,14},{12... | collective-permute-start | bytes 208904 | tf_op jit(solution)/shard_map/ppermute | solution.py:235
  17.4 6.2 %collective-permute-start.3 = (bf16[17,16,128]{2,1,0:T(8,128)(2,1)S(1)}, bf16[17,16,128]{2,1,0:T(8,128)(2,1)S(1)}, u32[]{:S(2)}, u32[]{:S(2)}) collective-permute-start(bf16[17,16,128]{2,1,0:T(8,128)(2,1)S(1)} %shard_map.93.refs_0_), channel_id=1, source_target_pairs={{0,6},{2,4},{4,2},{6,0},{1,7},{3,5},{5,3},{7,1},{8,14},{10,12},{12... | collective-permute-start | bytes 208904 | tf_op jit(solution)/shard_map/ppermute | solution.py:235
  24.3 1.2 %collective-permute-start.6 = (f32[16,512]{1,0:T(8,128)S(1)}, f32[16,512]{1,0:T(8,128)S(1)}, u32[]{:S(2)}, u32[]{:S(2)}) collective-permute-start(f32[16,512]{1,0:T(8,128)S(1)} %get-tuple-element.18), channel_id=1, source_target_pairs={{0,1},{1,0},{2,3},{3,2},{4,5},{5,4},{6,7},{7,6},{8,9},{9,8},{10,11... | collective-permute-start | bytes 98312 | tf_op jit(solution)/shard_map/ppermute | solution.py:310
